TPU v7x, 32 devices: a whole 2x2x4 slice. The times are simulated.
32 devices in a mesh: ep: 8 (over z, x), tp: 4 (over y, core).
Axes of the slice: x: 2, y: 2, z: 4, core: 2. Of those that a mesh axis runs over, the one named last changes fastest.
Arguments:
- tokens: bfloat16 [384, 2048], P('ep'), may hold values from -6 to 6
- state: float32 [384, 8, 128, 128], P('ep', 'tp'), may hold values from -4 to 4
- norm_gain: float32 [2048], replicated, may hold values from 0.1 to 1.9
- w_query: bfloat16 [2048, 1024], P('ep', 'tp'), may hold values from -0.125 to 0.125
- w_forget: bfloat16 [2048, 1024], P('ep', 'tp'), may hold values from -0.125 to 0.125
- w_input: bfloat16 [2048, 1024], P('ep', 'tp'), may hold values from -0.125 to 0.125
- w_outgate: bfloat16 [2048, 1024], P('ep', 'tp'), may hold values from -0.125 to 0.125
- lower_bound: float32 [1024], P('tp'), may hold values from 0 to 0.9
- head_gain: float32 [1024], P('tp'), may hold values from 0.1 to 1.9
- w_output: bfloat16 [1024, 2048], P('tp'), may hold values from -0.1875 to 0.1875
- ffn_gain: float32 [2048], replicated, may hold values from 0.1 to 1.9
- route_ids: int32 [384, 4], P('ep'), may hold values from 0 to 15, all different within a row; in each aligned block of 48 rows (0 to 47, 48 to 95, ...) at most 24 rows name the same one
- route_weight: float32 [384, 4], P('ep'), may hold values from 0.2 to 1
- expert_gate: bfloat16 [16, 2048, 1024], P('ep', None, 'tp'), may hold values from -0.125 to 0.125
- expert_up: bfloat16 [16, 2048, 1024], P('ep', None, 'tp'), may hold values from -0.125 to 0.125
- expert_down: bfloat16 [16, 1024, 2048], P('ep', 'tp'), may hold values from -0.1875 to 0.1875
- shared_gate: bfloat16 [2048, 1024], P(None, 'tp'), may hold values from -0.125 to 0.125
- shared_up: bfloat16 [2048, 1024], P(None, 'tp'), may hold values from -0.125 to 0.125
- shared_down: bfloat16 [1024, 2048], P('tp'), may hold values from -0.1875 to 0.1875
- dense_gate: bfloat16 [2048, 8192], P('tp', 'ep'), may hold values from -0.125 to 0.125
- dense_up: bfloat16 [2048, 8192], P('tp', 'ep'), may hold values from -0.125 to 0.125
- dense_down: bfloat16 [8192, 2048], P('ep', 'tp'), may hold values from -0.0625 to 0.0625
- dense_mix: float32 [2048], P('tp'), may hold values from -6 to 6
Outputs:
- mixed: bfloat16 [384, 2048], P('ep', 'tp')
- new_state: float32 [384, 8, 128, 128], P('ep', 'tp')
Inputs may be any that keep to these rules, and one draw needn't show every extreme that they name: `route_ids`: each row names 4 different experts. Among the rows of one device no expert is named more than 24 times, and in every draw some expert is named exactly 24 times by some device's rows.
All inputs are finite; a program needn't handle non-finite values.
Results may differ from a plain program's by a relative error of at most 0.025.
Values may be sent and summed in bfloat16 or wider, within the bound.
A program may use at most 64 MiB of HBM per device.

v0:
```python
import jax
import jax.numpy as jnp
from jax import lax
from jax.sharding import PartitionSpec as P

EPS = 1e-06


def rms_scale(values, gain):
    values = values.astype(jnp.float32)
    return values * lax.rsqrt(jnp.mean(values * values, axis=-1, keepdims=True) + EPS) * gain


def rounded(values):
    return lax.optimization_barrier(values.astype(jnp.bfloat16)).astype(jnp.float32)


def local(
    tokens,
    state,
    norm_gain,
    w_query,
    w_forget,
    w_input,
    w_outgate,
    lower_bound,
    head_gain,
    w_output,
    ffn_gain,
    route_ids,
    route_weight,
    expert_gate,
    expert_up,
    expert_down,
    shared_gate,
    shared_up,
    shared_down,
    dense_gate,
    dense_up,
    dense_down,
    dense_mix,
):
    ep_size = lax.axis_size("ep")
    tp_size = lax.axis_size("tp")
    seq_local, width = tokens.shape
    mix_local = w_query.shape[1]
    heads_local = state.shape[1]
    head_dim = state.shape[2]
    width_local = width // tp_size
    tp_index = lax.axis_index("tp")
    normed = rms_scale(tokens, norm_gain).astype(jnp.bfloat16)
    columns = lax.all_to_all(normed, "ep", split_axis=1, concat_axis=0, tiled=True)
    joined = jnp.concatenate([w_query, w_forget, w_input, w_outgate], axis=1)
    block = columns
    projected = lax.psum_scatter(
        jnp.dot(block, joined, preferred_element_type=jnp.float32).astype(jnp.bfloat16),
        "ep",
        scatter_dimension=0,
        tiled=True,
    ).astype(jnp.float32)
    projected = rounded(projected)
    query, forget_pre, values, out_gate = jnp.split(projected, 4, axis=1)
    shape = (seq_local, heads_local, head_dim)
    forget_sig = jax.nn.sigmoid(forget_pre)
    decay = (lower_bound + (1.0 - lower_bound) * forget_sig).reshape(shape)
    keygate = ((1.0 - lower_bound) * (1.0 - forget_sig)).reshape(shape)
    new_state = decay[..., None] * state + keygate[..., None] * values.reshape(shape)[:, :, None, :]
    readout = jnp.einsum(
        "bhk,bhkv->bhv", query.reshape(shape), new_state, precision=lax.Precision.HIGHEST
    )
    readout = readout * lax.rsqrt(jnp.mean(readout * readout, axis=-1, keepdims=True) + EPS)
    head_out = (readout.reshape(seq_local, mix_local) * head_gain * jax.nn.silu(out_gate)).astype(
        jnp.bfloat16
    )
    head_part = rounded(jnp.dot(head_out, w_output, preferred_element_type=jnp.float32))
    resid = tokens.astype(jnp.float32) + lax.psum(head_part.astype(jnp.bfloat16), "tp").astype(
        jnp.float32
    )
    moe_in = rms_scale(resid, ffn_gain).astype(jnp.bfloat16)
    exp_local = expert_gate.shape[0]
    experts = exp_local * ep_size
    topk = route_ids.shape[1]
    capacity = max(2, 2 * seq_local * topk // experts)
    flat_ids = route_ids.reshape(-1)
    onehot = (flat_ids[:, None] == jnp.arange(experts, dtype=jnp.int32)[None, :]).astype(jnp.int32)
    slot_rank = jnp.sum((jnp.cumsum(onehot, axis=0) - onehot) * onehot, axis=1)
    slot_index = (flat_ids * capacity + slot_rank).reshape(seq_local, topk)
    slot_ids = jnp.arange(experts * capacity, dtype=jnp.int32)
    slot_hits = slot_index[None, :, :] == slot_ids[:, None, None]
    dispatch = jnp.sum(slot_hits.astype(jnp.bfloat16), axis=2)
    outgoing = jnp.dot(dispatch, moe_in, preferred_element_type=jnp.float32).astype(jnp.bfloat16)
    outgoing = outgoing.reshape(experts, capacity, width)
    incoming = lax.all_to_all(outgoing, "ep", split_axis=0, concat_axis=0, tiled=True)
    count = incoming.shape[1]
    grouped = incoming.reshape(ep_size, exp_local, count, width)
    gate_pre = jnp.einsum(
        "sexd,edf->sexf", grouped, expert_gate, preferred_element_type=jnp.float32
    )
    up_pre = jnp.einsum("sexd,edf->sexf", grouped, expert_up, preferred_element_type=jnp.float32)
    hidden = (jax.nn.silu(gate_pre) * up_pre).astype(jnp.bfloat16)
    partial_value = rounded(
        jnp.einsum("sexf,efd->sexd", hidden, expert_down, preferred_element_type=jnp.float32)
    )
    summed = lax.psum_scatter(
        partial_value.astype(jnp.bfloat16), "tp", scatter_dimension=3, tiled=True
    )
    results = lax.all_to_all(
        summed.reshape(experts, count, width_local), "ep", split_axis=0, concat_axis=0, tiled=True
    )
    combine = jnp.sum(
        jnp.where(
            slot_index[:, :, None] == slot_ids[None, None, :],
            route_weight[:, :, None],
            jnp.float32(0.0),
        ),
        axis=1,
    )
    routed = jnp.dot(
        combine,
        results.reshape(experts * capacity, width_local).astype(jnp.float32),
        precision=lax.Precision.HIGHEST,
    )
    shared_hidden = (
        jax.nn.silu(jnp.dot(moe_in, shared_gate, preferred_element_type=jnp.float32))
        * jnp.dot(moe_in, shared_up, preferred_element_type=jnp.float32)
    ).astype(jnp.bfloat16)
    shared_part = rounded(jnp.dot(shared_hidden, shared_down, preferred_element_type=jnp.float32))
    shared_out = lax.psum_scatter(
        shared_part.astype(jnp.bfloat16), "tp", scatter_dimension=1, tiled=True
    ).astype(jnp.float32)
    own_columns = lax.dynamic_slice_in_dim(moe_in, tp_index * width_local, width_local, 1)
    dense_joined = jnp.concatenate([dense_gate, dense_up], axis=1)
    dense_pre = jnp.dot(
        lax.all_gather(own_columns, "ep", axis=0, tiled=True),
        dense_joined,
        preferred_element_type=jnp.float32,
    )
    dense_pre = lax.psum(rounded(dense_pre).astype(jnp.bfloat16), "tp").astype(jnp.float32)
    dense_pre_gate, dense_pre_up = jnp.split(dense_pre, 2, axis=1)
    dense_hidden = (jax.nn.silu(dense_pre_gate) * dense_pre_up).astype(jnp.bfloat16)
    block = dense_hidden
    dense_out = lax.psum_scatter(
        jnp.dot(block, dense_down, preferred_element_type=jnp.float32).astype(jnp.bfloat16),
        "ep",
        scatter_dimension=0,
        tiled=True,
    ).astype(jnp.float32)
    own_resid = lax.dynamic_slice_in_dim(resid, tp_index * width_local, width_local, 1)
    mixed = (own_resid + routed + shared_out + jax.nn.sigmoid(dense_mix) * dense_out).astype(
        jnp.bfloat16
    )
    return (mixed, new_state)


def solution(mesh):
    placed = (
        P("ep", None),
        P("ep", "tp", None, None),
        P(),
        P("ep", "tp"),
        P("ep", "tp"),
        P("ep", "tp"),
        P("ep", "tp"),
        P("tp"),
        P("tp"),
        P("tp", None),
        P(),
        P("ep", None),
        P("ep", None),
        P("ep", None, "tp"),
        P("ep", None, "tp"),
        P("ep", "tp", None),
        P(None, "tp"),
        P(None, "tp"),
        P("tp", None),
        P("tp", "ep"),
        P("tp", "ep"),
        P("ep", "tp"),
        P("tp"),
    )
    return jax.shard_map(
        local,
        mesh=mesh,
        in_specs=placed,
        out_specs=(P("ep", "tp"), P("ep", "tp", None, None)),
        check_vma=False,
    )
```

profile of v0, /device:TPU:0, one launch (start us, length us, event | category | flops | bytes accessed | tf_op | source)
XLA Modules:
  0.0 373.1 jit_solution(8439194973231213220)
XLA Ops:
  7.2 0.0 copy-start
  7.2 0.0 reduce-scatter.5.cloned.1.call-start
  7.2 1.2 fusion.48
  8.4 1.1 fusion.50
  9.5 0.0 copy-start.6
  9.5 0.0 copy-start.7
  9.6 15.0 %all_to_all.29 = bf16[48,8,256]{2,0,1:T(8,128)(2,1)S(1)} all-to-all(bf16[48,8,256]{2,0,1:T(8,128)(2,1)S(1)} %bitcast.88), channel_id=1, replica_groups=mesh['ep'=8,'tp'=4] {'ep'}, dimensions={1} | all-to-all | bytes 393216 | tf_op jit(solution)/shard_map/all_to_all | solution.py:52
  24.6 2.3 convolution_convert_fusion.5
  26.9 0.0 reduce-scatter.5.cloned.1.call-update
  27.0 0.0 all-reduce.4.cloned.1.call-start
  27.0 0.1 copy.60
  27.1 0.1 eq.48
  27.2 0.6 reduce-window.6
  27.8 0.2 slice_reduce_fusion
  28.1 0.1 bitcast_bitcast_fusion
  28.2 0.1 reduce_sum.62
  28.3 0.1 copy.63
  28.4 60.6 %reduce-scatter.5.cloned.1.call-done = bf16[48,1024]{1,0:T(8,128)(2,1)} async-done(((bf16[384,1024]{1,0:T(8,128)(2,1)}), bf16[48,1024]{1,0:T(8,128)(2,1)}) %reduce-scatter.5.cloned.1.call-update) | async-done | bytes 98320 | tf_op jit(solution)/shard_map/reduce_scatter | solution.py:55
  89.0 0.9 convert_element_type.87
  89.9 0.7 split.26
  90.7 0.7 split.24
  91.5 7.1 %multiply_add_fusion = f32[48,2,128,128]{3,2,1,0:T(8,128)S(1)} fusion(f32[48,2,128,128]{3,2,1,0:T(8,128)} %param.24, f32[48,2,128]{2,1,0:T(2,128)S(1)} %mul.163, f32[48,2,128]{2,1,0:T(2,128)S(1)} %mul.161, f32[48,2,128]{2,1,0:T(2,128)S(1)} %mul.157), kind=kLoop, calls=%fused_computation | loop fusion | flops 4718592 | bytes 12730368 | tf_op jit(solution)/shard_map/add | solution.py:67
  98.7 0.0 copy-start.1
  98.7 0.0 copy-start.4
  98.7 0.0 copy-start.10
  98.7 0.0 copy-start.2
  98.7 3.0 fusion.81
  101.7 0.1 multiply_reduce_fusion.1
  101.8 0.1 broadcast_multiply_fusion
  102.0 1.0 convolution_convert_fusion.4
  102.9 0.0 all-reduce.4.cloned.1.call-update
  103.0 0.1 fusion.58
  103.1 31.1 %all-reduce.4.cloned.1.call-done = bf16[48,2048]{1,0:T(8,128)(2,1)} async-done(((bf16[48,2048]{1,0:T(8,128)(2,1)}), bf16[48,2048]{1,0:T(8,128)(2,1)}) %all-reduce.4.cloned.1.call-update) | async-done | bytes 196624 | tf_op jit(solution)/shard_map/psum | solution.py:76
  134.2 1.9 convert_add_fusion
  136.1 1.0 multiply_convert_fusion
  137.1 1.7 convolution_convert_fusion
  138.8 5.6 %all-to-all-start.1 = ((bf16[16,24,2048]{2,1,0:T(8,128)(2,1)}), bf16[16,24,2048]{2,1,0:T(8,128)(2,1)}, u32[]{:S(2)}, u32[]{:S(2)}) async-start(bf16[16,24,2048]{2,1,0:T(8,128)(2,1)} %bitcast.85), calls=%async_computation.2 | async-start | bytes 3145728 | tf_op jit(solution)/shard_map/all_to_all | solution.py:93
  144.5 0.0 all-reduce.6.cloned.1.call-start
  144.5 56.7 %all_gather.3 = bf16[384,512]{1,0:T(8,128)(2,1)S(1)} all-gather(bf16[48,512]{1,0:T(8,128)(2,1)S(1)} %constant_dynamic-slice_fusion), channel_id=1, replica_groups=mesh['ep'=8,'tp'=4] {'ep'}, dimensions={0}, use_global_device_ids=true | all-gather | bytes 442368 | tf_op jit(solution)/shard_map/all_gather | solution.py:134
  201.2 3.3 convolution_convert_fusion.1
  204.5 0.0 all-reduce.6.cloned.1.call-update
  204.6 0.0 reduce-scatter.7.cloned.1.call-start
  204.6 0.0 all-to-all-done.1
  204.6 3.4 fusion.12
  208.1 4.7 %fusion = bf16[8,2,24,2048]{3,2,0,1:T(8,128)(2,1)} fusion(bf16[2,256,2048]{2,1,0:T(8,128)(2,1)S(1)} %copy-done, bf16[2,2048,256]{2,1,0:T(8,128)(2,1)} %param.37, bf16[8,2,24,2048]{3,2,1,0:T(8,128)(2,1)} %bitcast.6, f32[8,2,24,256]{3,2,0,1:T(8,128)} %fusion.12), kind=kOutput, calls=%fused_computation.4 | convolution fusion | flops 806682624 | bytes 7733248 | tf_op jit(solution)/shard_map/sexf,efd->sexd/dot_general | solution.py:102
  212.8 0.0 reduce-scatter.7.cloned.1.call-update
  212.8 0.0 reduce-scatter.9.cloned.1.call-start
  212.8 0.3 fusion.82
  213.1 3.0 convolution_convert_fusion.3
  216.1 0.0 reduce-scatter.9.cloned.1.call-update
  216.2 0.0 reduce-scatter.11.cloned.1.call-start
  216.2 30.1 %all-reduce.6.cloned.1.call-done = bf16[384,2048]{1,0:T(8,128)(2,1)} async-done(((bf16[384,2048]{1,0:T(8,128)(2,1)}), bf16[384,2048]{1,0:T(8,128)(2,1)}) %all-reduce.6.cloned.1.call-update) | async-done | bytes 1572880 | tf_op jit(solution)/shard_map/psum | solution.py:138
  246.4 1.8 convert_element_type.102
  248.1 0.0 copy-start.8
  248.1 0.0 copy-start.9
  248.2 2.6 convolution_convert_fusion.6
  250.8 0.0 reduce-scatter.11.cloned.1.call-update
  250.8 26.1 %reduce-scatter.7.cloned.1.call-done = bf16[8,2,24,512]{3,2,0,1:T(8,128)(2,1)} async-done(((bf16[8,2,24,2048]{3,2,0,1:T(8,128)(2,1)}), bf16[8,2,24,512]{3,2,0,1:T(8,128)(2,1)}) %reduce-scatter.7.cloned.1.call-update) | async-done | bytes 393232 | tf_op jit(solution)/shard_map/reduce_scatter | solution.py:104
  276.9 1.8 copy.66
  278.7 5.5 %all-to-all-start.2 = ((bf16[16,24,512]{2,1,0:T(8,128)(2,1)}), bf16[16,24,512]{2,1,0:T(8,128)(2,1)S(1)}, u32[]{:S(2)}, u32[]{:S(2)}) async-start(bf16[16,24,512]{2,1,0:T(8,128)(2,1)} %bitcast.16), calls=%async_computation.4 | async-start | bytes 786432 | tf_op jit(solution)/shard_map/all_to_all | solution.py:107
  284.2 0.1 select_reduce_fusion
  284.4 14.6 %reduce-scatter.9.cloned.1.call-done = bf16[48,512]{1,0:T(8,128)(2,1)} async-done(((bf16[48,2048]{1,0:T(8,128)(2,1)}), bf16[48,512]{1,0:T(8,128)(2,1)}) %reduce-scatter.9.cloned.1.call-update) | async-done | bytes 49168 | tf_op jit(solution)/shard_map/reduce_scatter | solution.py:128
  299.0 65.3 %reduce-scatter.11.cloned.1.call-done = bf16[48,512]{1,0:T(8,128)(2,1)} async-done(((bf16[384,512]{1,0:T(8,128)(2,1)}), bf16[48,512]{1,0:T(8,128)(2,1)}) %reduce-scatter.11.cloned.1.call-update) | async-done | bytes 49168 | tf_op jit(solution)/shard_map/reduce_scatter | solution.py:142
  364.3 1.9 fusion.34
  (34 shorter events, 0.3 us)
Async XLA Ops:
  7.2 200.9 %copy-start = (bf16[2,256,2048]{2,1,0:T(8,128)(2,1)S(1)}, bf16[2,256,2048]{2,1,0:T(8,128)(2,1)}, u32[]{:S(2)}) copy-start(bf16[2,256,2048]{2,1,0:T(8,128)(2,1)} %param.38) | copy-start | bytes 6291460
  7.2 81.8 %reduce-scatter.5.cloned.1.call-start = ((), (), s32[]{:S(2)}) async-start(), calls=%async_computation.7 | async-start | bytes 884736 | tf_op jit(solution)/shard_map/reduce_scatter | solution.py:55
  9.5 17.5 %copy-start.6 = (s32[48,4]{0,1:T(4,128)S(1)}, s32[48,4]{0,1:T(4,128)}, u32[]{:S(2)}) copy-start(s32[48,4]{0,1:T(4,128)} %param.34) | copy-start | bytes 2308
  9.5 18.8 %copy-start.7 = (f32[256]{0:T(256)S(1)}, f32[256]{0:T(256)}, u32[]{:S(2)}) copy-start(f32[256]{0:T(256)} %param.30) | copy-start | bytes 3076
  27.0 107.2 %all-reduce.4.cloned.1.call-start = ((), (), s32[]{:S(2)}) async-start(), calls=%async_computation.8 | async-start | bytes 393216 | tf_op jit(solution)/shard_map/psum | solution.py:76
  98.7 3.0 copy-start.1
  98.7 3.3 copy-start.4
  98.7 3.3 copy-start.10
  98.7 35.5 %copy-start.2 = (bf16[48,2048]{1,0:T(8,128)(2,1)S(1)}, bf16[48,2048]{1,0:T(8,128)(2,1)}, u32[]{:S(2)}) copy-start(bf16[48,2048]{1,0:T(8,128)(2,1)} %param.23) | copy-start | bytes 589828
  101.7 34.4 %copy-start.5 = (f32[2048]{0:T(1024)S(1)}, f32[2048]{0:T(1024)}, u32[]{:S(2)}) copy-start(f32[2048]{0:T(1024)} %param.33) | copy-start | bytes 24580
  138.8 62.4 %copy-start.11 = (bf16[512,1024]{1,0:T(8,128)(2,1)S(1)}, bf16[512,1024]{1,0:T(8,128)(2,1)}, u32[]{:S(2)}) copy-start(bf16[512,1024]{1,0:T(8,128)(2,1)} %param.43) | copy-start | bytes 3145732
  138.8 65.8 %all-to-all-start.1 = ((bf16[16,24,2048]{2,1,0:T(8,128)(2,1)}), bf16[16,24,2048]{2,1,0:T(8,128)(2,1)}, u32[]{:S(2)}, u32[]{:S(2)}) async-start(bf16[16,24,2048]{2,1,0:T(8,128)(2,1)} %bitcast.85), calls=%async_computation.2 | async-start | bytes 3145728 | tf_op jit(solution)/shard_map/all_to_all | solution.py:93
  144.5 101.9 %all-reduce.6.cloned.1.call-start = ((), (), s32[]{:S(2)}) async-start(), calls=%async_computation.11 | async-start | bytes 3145728 | tf_op jit(solution)/shard_map/psum | solution.py:138
  204.6 72.3 %reduce-scatter.7.cloned.1.call-start = ((), (), s32[]{:S(2)}) async-start(), calls=%async_computation.9 | async-start | bytes 1966080 | tf_op jit(solution)/shard_map/reduce_scatter | solution.py:104
  208.1 4.8 %copy-start.3 = (bf16[2048,256]{1,0:T(8,128)(2,1)S(1)}, bf16[2048,256]{1,0:T(8,128)(2,1)}, u32[]{:S(2)}) copy-start(bf16[2048,256]{1,0:T(8,128)(2,1)} %param.39) | copy-start | bytes 3145732
  212.8 86.2 %reduce-scatter.9.cloned.1.call-start = ((), (), s32[]{:S(2)}) async-start(), calls=%async_computation.10 | async-start | bytes 245760 | tf_op jit(solution)/shard_map/reduce_scatter | solution.py:128
  216.2 148.2 %reduce-scatter.11.cloned.1.call-start = ((), (), s32[]{:S(2)}) async-start(), calls=%async_computation.12 | async-start | bytes 442368 | tf_op jit(solution)/shard_map/reduce_scatter | solution.py:142
  248.1 36.1 %copy-start.8 = (f32[48,4]{0,1:T(4,128)S(1)}, f32[48,4]{0,1:T(4,128)}, u32[]{:S(2)}) copy-start(f32[48,4]{0,1:T(4,128)} %param.35) | copy-start | bytes 2308
  248.1 36.2 %copy-start.9 = (f32[512]{0:T(512)S(1)}, f32[512]{0:T(512)}, u32[]{:S(2)}) copy-start(f32[512]{0:T(512)} %param.45) | copy-start | bytes 6148
  278.7 85.7 %all-to-all-start.2 = ((bf16[16,24,512]{2,1,0:T(8,128)(2,1)}), bf16[16,24,512]{2,1,0:T(8,128)(2,1)S(1)}, u32[]{:S(2)}, u32[]{:S(2)}) async-start(bf16[16,24,512]{2,1,0:T(8,128)(2,1)} %bitcast.16), calls=%async_computation.4 | async-start | bytes 786432 | tf_op jit(solution)/shard_map/all_to_all | solution.py:107
Sparse Core Ops, SparseCore 0:
  27.1 61.8 reduce-scatter.4
  103.1 31.0 all-reduce.3
  204.7 41.6 all-reduce.5
  248.7 28.0 reduce-scatter.6
  279.2 19.7 reduce-scatter.8
  302.1 62.1 reduce-scatter.10
where the time goes:
time: 374 us; the launch traced here: 373 us
  waiting for transfers between devices  228 us (61%)
  blocking collectives  71.7 us (19%)
  matrix products  27.3 us (7%)
  other arithmetic  16.2 us (4%)
  between operations  14.4 us (4%)
  starting transfers between devices  11.4 us (3%)
  local copies, waits for them, and re-layouts  4.04 us (1%)
    reduce_scatter x1, waiting for transfers between devices, local(): lax.psum_scatter(jnp.dot(block, dense_down, preferred_element_type=jnp.fl...  65.3 us
    reduce_scatter x1, waiting for transfers between devices, local(): lax.psum_scatter(jnp.dot(block, joined, preferred_element_type=jnp.float3...  60.6 us
    all_gather x1, blocking collectives, local(): lax.all_gather(own_columns, 'ep', axis=0, tiled=True)  56.7 us
    psum x1, waiting for transfers between devices, local(): lax.psum(head_part.astype(jnp.bfloat16), 'tp').astype(jnp.float32)  31.1 us
    psum x1, waiting for transfers between devices, local(): lax.psum(rounded(dense_pre).astype(jnp.bfloat16), 'tp').astype(jnp.float32)  30.1 us
    reduce_scatter x1, waiting for transfers between devices, local(): lax.psum_scatter(partial_value.astype(jnp.bfloat16), 'tp', scatter_dimens...  26.1 us
    all_to_all x1, blocking collectives, local(): lax.all_to_all(normed, 'ep', split_axis=1, concat_axis=0, tiled=True)  15 us
    reduce_scatter x1, waiting for transfers between devices, local(): lax.psum_scatter(shared_part.astype(jnp.bfloat16), 'tp', scatter_dimensio...  14.6 us
  transfers between devices with their start and end apart: 8, of which 6 were waited for; matrix products, arithmetic and copies ran while one was open for 6% of the time, Pallas kernels for 0%

commit v1 on v0

v1 whole, which is shorter than its diff:
```python
import functools

import jax
import jax.numpy as jnp
from jax import lax
from jax.experimental import pallas as pl
from jax.experimental.pallas import tpu as pltpu
from jax.sharding import PartitionSpec as P

EPS = 1e-06
LANES = 128
CORES = 2
F32 = jnp.float32
BF16 = jnp.bfloat16
VMEM_BYTES = 60 * 1024 * 1024


def send(src, dst, sems, slot, peer):
    send_sem, recv_sem = sems
    return pltpu.make_async_remote_copy(
        src_ref=src,
        dst_ref=dst,
        send_sem=send_sem.at[slot],
        recv_sem=recv_sem.at[slot],
        device_id=peer,
        device_id_type=pl.DeviceIdType.MESH,
    )


def span(index, size):
    return pl.ds(pl.multiple_of(index * size, size), size)


def greet(n, tpn, me, tp):
    barrier = pltpu.get_barrier_semaphore()
    for s in range(1, n):
        pl.semaphore_signal(
            barrier,
            inc=1,
            device_id={"ep": lax.rem(me + s, n)},
            device_id_type=pl.DeviceIdType.MESH,
        )
    for s in range(1, tpn):
        pl.semaphore_signal(
            barrier,
            inc=1,
            device_id={"tp": lax.rem(tp + s, tpn)},
            device_id_type=pl.DeviceIdType.MESH,
        )
    pl.semaphore_wait(barrier, n - 1 + tpn - 1)


def front_kernel(n, tpn, move, *refs):
    tokens, gain, route, mix, wq, wf, wi, wo = refs[:8]
    refs = refs[8:]
    if move:
        dgate, dup, ddown = refs[:3]
        refs = refs[3:]
    proj, route_all, mix_all = refs[:3]
    refs = refs[3:]
    if move:
        gate_out, up_out, down_out = refs[:3]
        refs = refs[3:]
    nsend, ncol, psend, precv = refs[:4]
    nsems, rsems, psems, msems = [(refs[4 + 2 * i], refs[5 + 2 * i]) for i in range(4)]
    refs = refs[12:]
    me = lax.axis_index("ep")
    tp = lax.axis_index("tp")
    seq = tokens.shape[0]
    depth = wq.shape[0]
    mixw = wq.shape[1]
    x = tokens[...].astype(F32)
    normed = (
        x * lax.rsqrt(jnp.mean(x * x, axis=-1, keepdims=True) + EPS) * gain[...]
    ).astype(BF16)
    for d in range(n):
        nsend[d] = normed[:, d * depth : (d + 1) * depth]
    greet(n, tpn, me, tp)
    ncopies, others = [None], []
    for s in range(1, n):
        peer = lax.rem(me + s, n)
        copy = send(nsend.at[peer], ncol.at[me], nsems, s, {"ep": peer})
        copy.start()
        ncopies.append(copy)
    if move:
        wsems = (refs[0], refs[1])
        lsems = refs[2]
        rows = dgate.shape[0]
        cols = gate_out.shape[1]
        drows = down_out.shape[0]
        dcols = ddown.shape[1]
        locals_ = []
        for s in range(tpn):
            peer = lax.rem(tp + s, tpn)
            for i, (a, b) in enumerate(
                (
                    (dgate.at[:, span(peer, cols)], gate_out.at[span(tp, rows), :]),
                    (dup.at[:, span(peer, cols)], up_out.at[span(tp, rows), :]),
                    (ddown.at[span(peer, drows), :], down_out.at[:, span(tp, dcols)]),
                )
            ):
                if s == 0:
                    copy = pltpu.make_async_copy(a, b, lsems.at[i])
                    locals_.append(copy)
                else:
                    copy = send(a, b, wsems, i * tpn + s, {"tp": peer})
                    others.append(copy)
                copy.start()
    for s in range(1, tpn):
        copy = send(mix, mix_all.at[tp], msems, s, {"tp": lax.rem(tp + s, tpn)})
        copy.start()
        others.append(copy)
    for s in range(1, n):
        copy = send(route, route_all.at[me], rsems, s, {"ep": lax.rem(me + s, n)})
        copy.start()
        others.append(copy)
    mix_all[tp] = mix[...]
    route_all[me] = route[...]

    def project(block):
        return [
            jnp.dot(block, w[...], preferred_element_type=F32).astype(BF16)
            for w in (wq, wf, wi, wo)
        ]

    pcopies = [None]
    for s in range(1, n):
        source = lax.rem(me + n - s, n)
        ncopies[s].wait_recv()
        for i, part in enumerate(project(ncol[source])):
            psend[source, :, i * mixw : (i + 1) * mixw] = part
        copy = send(psend.at[source], precv.at[me], psems, s, {"ep": source})
        copy.start()
        pcopies.append(copy)
    own = jnp.concatenate(project(nsend[me]), axis=1).astype(F32)
    for s in range(1, n):
        pcopies[s].wait_recv()
        own = own + precv[lax.rem(me + s, n)].astype(F32)
    proj[...] = own.astype(BF16)
    for s in range(1, n):
        ncopies[s].wait_send()
        pcopies[s].wait_send()
    for copy in others:
        copy.wait()
    if move:
        for copy in locals_:
            copy.wait()


def gather_kernel(
    n, tpn, tokens, gain, head, wout, resid, moe, hsend, hrecv, sqsend, sqrecv, *sems
):
    hsems, qsems, esems, ysems, csems = [(sems[2 * i], sems[2 * i + 1]) for i in range(5)]
    me = lax.axis_index("ep")
    tp = lax.axis_index("tp")
    seq, width = tokens.shape
    cols = width // tpn
    side, core = lax.div(tp, CORES), lax.rem(tp, CORES)
    sides = tpn // CORES
    twin = side * CORES + (CORES - 1 - core)
    for t in range(tpn):
        hsend[t] = jnp.dot(
            head[...], wout[:, t * cols : (t + 1) * cols], preferred_element_type=F32
        ).astype(BF16)
    greet(n, tpn, me, tp)
    hcopies = []
    for s in range(1, tpn):
        peer = lax.rem(tp + s, tpn)
        copy = send(hsend.at[peer], hrecv.at[tp], hsems, s, {"tp": peer})
        copy.start()
        hcopies.append(copy)
    total = hsend[tp].astype(F32)
    for s in range(1, tpn):
        hcopies[s - 1].wait_recv()
        total = total + hrecv[lax.rem(tp + tpn - s, tpn)].astype(F32)
    mine = span(tp, cols)
    total = tokens[:, mine].astype(F32) + total
    resid[...] = total
    square = jnp.broadcast_to(jnp.sum(total * total, axis=-1, keepdims=True), (seq, LANES))
    sqsend[...] = square
    qcopies = []
    for s in range(1, tpn):
        copy = send(sqsend, sqrecv.at[tp], qsems, s, {"tp": lax.rem(tp + s, tpn)})
        copy.start()
        qcopies.append(copy)
    for s in range(1, tpn):
        qcopies[s - 1].wait_recv()
        square = square + sqrecv[lax.rem(tp + tpn - s, tpn)]
    scale = lax.rsqrt(square[:, :1] / width + EPS)
    moe[span(me, seq), mine] = (total * scale * gain[:, mine]).astype(BF16)

    def block(e, t):
        return moe.at[span(e, seq), span(t, cols)]

    copies = []
    ecopies = [None]
    for s in range(1, n):
        copy = send(block(me, tp), block(me, tp), esems, s, {"ep": lax.rem(me + s, n)})
        copy.start()
        ecopies.append(copy)
    ycopies, ccopies = {}, {}
    for s in range(n):
        e = lax.rem(me + n - s, n)
        if s:
            ecopies[s].wait_recv()
        for q in range(1, sides):
            peer = lax.rem(side + q, sides) * CORES + core
            copy = send(block(e, tp), block(e, tp), ysems, s * sides + q, {"tp": peer})
            copy.start()
            ycopies[s, q] = copy
        copy = send(block(e, tp), block(e, tp), csems, s * sides, {"tp": twin})
        copy.start()
        ccopies[s, 0] = copy
    for s in range(n):
        e = lax.rem(me + n - s, n)
        for q in range(1, sides):
            ycopies[s, q].wait_recv()
            t = lax.rem(side + sides - q, sides) * CORES + core
            copy = send(block(e, t), block(e, t), csems, s * sides + q, {"tp": twin})
            copy.start()
            ccopies[s, q] = copy
    for copy in ccopies.values():
        copy.wait()
    for copy in list(ycopies.values()) + ecopies[1:] + hcopies + qcopies:
        copy.wait_send()


def reduce_kernel(
    n, tpn, part, shared, resid, out, crecv, ysend, yrecv, esend, erecv, *sems
):
    csems, ysems, esems = [(sems[2 * i], sems[2 * i + 1]) for i in range(3)]
    me = lax.axis_index("ep")
    tp = lax.axis_index("tp")
    seq, cols = resid.shape
    side, core = lax.div(tp, CORES), lax.rem(tp, CORES)
    sides = tpn // CORES
    twin = side * CORES + (CORES - 1 - core)
    greet(n, tpn, me, tp)
    order = list(range(1, n)) + [n, 0]

    def block(s, t):
        if s == n:
            return shared.at[:, span(t, cols)]
        return part.at[span(lax.rem(me + s, n), seq), span(t, cols)]

    turns = list(range(1, sides)) + [0]
    ccopies, ycopies, ecopies = {}, {}, {}
    for s in order:
        for q in turns:
            t = lax.rem(side + q, sides) * CORES + (CORES - 1 - core)
            i = s * sides + q
            copy = send(block(s, t), crecv.at[i], csems, i, {"tp": twin})
            copy.start()
            ccopies[s, q] = copy
    kept = {}
    for s in order:
        for q in turns[:-1]:
            peer = lax.rem(side + q, sides) * CORES + core
            i = s * sides + q
            ccopies[s, q].wait_recv()
            both = block(s, peer)[...].astype(F32) + crecv[i].astype(F32)
            ysend[i] = both.astype(BF16)
            copy = send(ysend.at[i], yrecv.at[i], ysems, i, {"tp": peer})
            copy.start()
            ycopies[s, q] = copy
    last = None
    for s in order:
        i = s * sides
        ccopies[s, 0].wait_recv()
        both = block(s, tp)[...].astype(F32) + crecv[i].astype(F32)
        for q in turns[:-1]:
            ycopies[s, q].wait_recv()
            both = both + yrecv[i + q].astype(F32)
        if 0 < s < n:
            esend[s] = both.astype(BF16)
            copy = send(esend.at[s], erecv.at[s], esems, s, {"ep": lax.rem(me + s, n)})
            copy.start()
            ecopies[s] = copy
        else:
            last = both if last is None else last + both
    last = last + resid[...]
    for s in range(1, n):
        ecopies[s].wait_recv()
        last = last + erecv[s].astype(F32)
    out[...] = last.astype(BF16)
    for group in (ccopies, ycopies, ecopies):
        for copy in group.values():
            copy.wait_send()


def pairs(counts):
    return [pltpu.SemaphoreType.DMA((c,)) for c in counts for _ in range(2)]


def call(kernel, outs, ins, spaces, out_spaces, scratch, ident):
    return pl.pallas_call(
        kernel,
        out_shape=outs,
        in_specs=[pl.BlockSpec(memory_space=s) for s in spaces],
        out_specs=[pl.BlockSpec(memory_space=s) for s in out_spaces],
        scratch_shapes=scratch,
        compiler_params=pltpu.CompilerParams(
            collective_id=ident, has_side_effects=True, vmem_limit_bytes=VMEM_BYTES
        ),
    )(*ins)


def local(
    tokens,
    state,
    norm_gain,
    w_query,
    w_forget,
    w_input,
    w_outgate,
    lower_bound,
    head_gain,
    w_output,
    ffn_gain,
    route_ids,
    route_weight,
    expert_gate,
    expert_up,
    expert_down,
    shared_gate,
    shared_up,
    shared_down,
    dense_gate,
    dense_up,
    dense_down,
    dense_mix,
):
    n = lax.axis_size("ep")
    tpn = lax.axis_size("tp")
    seq, width = tokens.shape
    depth, mix_local = w_query.shape
    heads_local = state.shape[1]
    head_dim = state.shape[2]
    cols = width // tpn
    exp_local = expert_gate.shape[0]
    experts = exp_local * n
    slots = -(-experts // LANES) * LANES
    sds = jax.ShapeDtypeStruct
    VM, ANY = pltpu.VMEM, pl.ANY

    route = jnp.sum(
        jnp.where(
            route_ids[:, :, None] == jnp.arange(slots, dtype=jnp.int32)[None, None, :],
            route_weight[:, :, None],
            jnp.float32(0.0),
        ),
        axis=1,
    )
    mix = jnp.broadcast_to(jax.nn.sigmoid(dense_mix)[None, :], (8, cols))
    dense_cols = dense_gate.shape[1] // tpn
    move = dense_cols % LANES == 0
    ins = [tokens, norm_gain[None, :], route, mix, w_query, w_forget, w_input, w_outgate]
    outs = [
        sds((seq, 4 * mix_local), BF16),
        sds((n, seq, slots), F32),
        sds((tpn, 8, cols), F32),
    ]
    scratch = [
        VM((n, seq, depth), BF16),
        VM((n, seq, depth), BF16),
        VM((n, seq, 4 * mix_local), BF16),
        VM((n, seq, 4 * mix_local), BF16),
    ] + pairs([n, n, n, tpn])
    spaces, out_spaces = [VM] * len(ins), [VM] * len(outs)
    if move:
        ins += [dense_gate, dense_up, dense_down]
        outs += [sds((width, dense_cols), BF16)] * 2 + [sds((dense_cols, width), BF16)]
        spaces += [ANY] * 3
        out_spaces += [ANY] * 3
        scratch += pairs([3 * tpn]) + [pltpu.SemaphoreType.DMA((3,))]
    res = call(
        functools.partial(front_kernel, n, tpn, move), outs, ins, spaces, out_spaces, scratch, 0
    )
    projected, route_all, mix_all = res[:3]
    if move:
        gate_w, up_w, down_w = res[3:]
    else:
        gate_w, up_w = [
            lax.all_to_all(w, "tp", split_axis=1, concat_axis=0, tiled=True)
            for w in (dense_gate, dense_up)
        ]
        down_w = lax.all_to_all(dense_down, "tp", split_axis=0, concat_axis=1, tiled=True)

    query, forget_pre, values, out_gate = jnp.split(projected.astype(F32), 4, axis=1)
    shape = (seq, heads_local, head_dim)
    forget_sig = jax.nn.sigmoid(forget_pre)
    decay = (lower_bound + (1.0 - lower_bound) * forget_sig).reshape(shape)
    keygate = ((1.0 - lower_bound) * (1.0 - forget_sig)).reshape(shape)
    new_state = decay[..., None] * state + keygate[..., None] * values.reshape(shape)[:, :, None, :]
    readout = jnp.einsum(
        "bhk,bhkv->bhv", query.reshape(shape), new_state, precision=lax.Precision.HIGHEST
    )
    readout = readout * lax.rsqrt(jnp.mean(readout * readout, axis=-1, keepdims=True) + EPS)
    head_out = (readout.reshape(seq, mix_local) * head_gain * jax.nn.silu(out_gate)).astype(BF16)

    sides = tpn // CORES
    resid, moe_in = call(
        functools.partial(gather_kernel, n, tpn),
        [sds((seq, cols), F32), sds((n * seq, width), BF16)],
        [tokens, ffn_gain[None, :], head_out, w_output],
        [VM] * 4,
        [VM] * 2,
        [
            VM((tpn, seq, cols), BF16),
            VM((tpn, seq, cols), BF16),
            VM((seq, LANES), F32),
            VM((tpn, seq, LANES), F32),
        ]
        + pairs([tpn, tpn, n, n * sides, n * sides]),
        1,
    )

    ep_index = lax.axis_index("ep")
    own = lax.dynamic_slice_in_dim(moe_in, ep_index * seq, seq, 0)
    shared_hidden = (
        jax.nn.silu(jnp.dot(own, shared_gate, preferred_element_type=F32))
        * jnp.dot(own, shared_up, preferred_element_type=F32)
    ).astype(BF16)
    shared_part = jnp.dot(shared_hidden, shared_down, preferred_element_type=F32).astype(BF16)

    route_rows = lax.dynamic_slice_in_dim(
        route_all.reshape(n * seq, slots), ep_index * exp_local, exp_local, 1
    )
    part = jnp.zeros((n * seq, width), F32)
    for e in range(exp_local):
        gate_pre = jnp.dot(moe_in, expert_gate[e], preferred_element_type=F32)
        up_pre = jnp.dot(moe_in, expert_up[e], preferred_element_type=F32)
        hidden = (jax.nn.silu(gate_pre) * up_pre * route_rows[:, e : e + 1]).astype(BF16)
        part = part + jnp.dot(hidden, expert_down[e], preferred_element_type=F32)
    dense_hidden = (
        jax.nn.silu(jnp.dot(moe_in, gate_w, preferred_element_type=F32))
        * jnp.dot(moe_in, up_w, preferred_element_type=F32)
    ).astype(BF16)
    mix_row = mix_all[:, 0, :].reshape(1, width)
    part = part + mix_row * jnp.dot(dense_hidden, down_w, preferred_element_type=F32)
    blocks = (n + 1) * sides
    (mixed,) = call(
        functools.partial(reduce_kernel, n, tpn),
        [sds((seq, cols), BF16)],
        [part.astype(BF16), shared_part, resid],
        [VM] * 3,
        [VM],
        [VM((blocks, seq, cols), BF16)] * 3 + [VM((n, seq, cols), BF16)] * 2
        + pairs([blocks, blocks, n]),
        2,
    )
    return (mixed, new_state)


def solution(mesh):
    placed = (
        P("ep", None),
        P("ep", "tp", None, None),
        P(),
        P("ep", "tp"),
        P("ep", "tp"),
        P("ep", "tp"),
        P("ep", "tp"),
        P("tp"),
        P("tp"),
        P("tp", None),
        P(),
        P("ep", None),
        P("ep", None),
        P("ep", None, "tp"),
        P("ep", None, "tp"),
        P("ep", "tp", None),
        P(None, "tp"),
        P(None, "tp"),
        P("tp", None),
        P("tp", "ep"),
        P("tp", "ep"),
        P("ep", "tp"),
        P("tp"),
    )
    return jax.shard_map(
        local,
        mesh=mesh,
        in_specs=placed,
        out_specs=(P("ep", "tp"), P("ep", "tp", None, None)),
        check_vma=False,
    )
```

time: 374 us -> 141 us (0.38)
  waiting for transfers between devices: 228 us -> 0 us
  Pallas kernels: 0 us -> 93.9 us
  blocking collectives: 71.7 us -> 0 us
  between operations: 14.4 us -> 0.85 us
  starting transfers between devices: 11.4 us -> 0 us
  other arithmetic: 16.2 us -> 11.1 us
    reduce_scatter x4 -> x0, waiting for transfers between devices: 167 us -> none  [the longest x1 65.3 us: local(): lax.psum_scatter(jnp.dot(block, dense_down, preferred_element_type=jnp.fl...]
    pallas_call x0 -> x3, Pallas kernels: none -> 93.9 us  [call(): pl.pallas_call(kernel, out_shape=outs, in_specs=[pl.BlockSpec(memory_spac...]
    psum x2 -> x0, waiting for transfers between devices: 61.2 us -> none  [the longest x1 31.1 us: local(): lax.psum(head_part.astype(jnp.bfloat16), 'tp').astype(jnp.float32)]
    all_gather x1 -> x0, blocking collectives: 56.7 us -> none  [local(): lax.all_gather(own_columns, 'ep', axis=0, tiled=True)]
    all_to_all x1 -> x0, blocking collectives: 15 us -> none  [local(): lax.all_to_all(normed, 'ep', split_axis=1, concat_axis=0, tiled=True)]
    all_to_all x2 -> x0, starting transfers between devices: 11.2 us -> none  [the longest x1 5.65 us: local(): lax.all_to_all(outgoing, 'ep', split_axis=0, concat_axis=0, tiled=True)]
    dot_general x10 -> x8, matrix products: 24.3 us -> 26.6 us  [the longest x2 10 us: local(): part = part + jnp.dot(hidden, expert_down[e], preferred_element_type=F32)]
  transfers between devices with their start and end apart: 8 -> 0, of which waited for: 6 -> 0; matrix products, arithmetic and copies ran while one was open for 6% -> 0% of each run, Pallas kernels for 0% -> 0%
where the time goes in v1:
time: 141 us; the launch traced here: 140 us
  Pallas kernels  93.9 us (67%)
  matrix products  29.6 us (21%)
  other arithmetic  11.1 us (8%)
  local copies, waits for them, and re-layouts  4.81 us (3%)
    pallas_call x3, Pallas kernels, call(): pl.pallas_call(kernel, out_shape=outs, in_specs=[pl.BlockSpec(memory_spac...  93.9 us
    dot_general x2, matrix products, local(): part = part + jnp.dot(hidden, expert_down[e], preferred_element_type=F32)  10 us
    add x1, other arithmetic, local(): decay[..., None] * state  7.12 us
    dot_general x1, matrix products, local(): jnp.dot(dense_hidden, down_w, preferred_element_type=F32)  6.42 us
    dot_general x2, matrix products, local(): gate_pre = jnp.dot(moe_in, expert_gate[e], preferred_element_type=F32)  4.2 us
    dot_general x1, matrix products, local(): jnp.einsum('bhk,bhkv->bhv', query.reshape(shape), new_state, precision=la...  2.96 us

profile of v1, /device:TPU:0, one launch (start us, length us, event | category | flops | bytes accessed | tf_op | source)
XLA Modules:
  0.0 140.2 jit_solution(10680880252173510638)
XLA Ops:
  0.6 0.0 copy-start
  0.6 1.5 %select_reduce_fusion.refs_2_ = f32[48,128]{1,0:T(8,128)} fusion(f32[48,4]{0,1:T(4,128)} %param.35, s32[48,4]{0,1:T(4,128)} %param.34), kind=kLoop, calls=%fused_computation.54 | loop fusion | flops 67584 | bytes 26112 | tf_op jit(solution)/shard_map/reduce_sum | solution.py:346
  2.2 0.7 add_divide_fusion
  2.8 0.6 broadcast_in_dim.36.refs_3_
  3.5 0.0 copy-start.4
  3.5 45.3 %shard_map.230 = (bf16[48,1024]{1,0:T(8,128)(2,1)}, f32[8,48,128]{2,1,0:T(8,128)}, f32[4,8,512]{2,1,0:T(8,128)}, bf16[2048,256]{1,0:T(8,128)(2,1)}, bf16[2048,25...) custom-call(bf16[48,2048]{1,0:T(8,128)(2,1)} %tokens.1, f32[1,2048]{1,0:T(1,128)} %bitcast.52, ...), custom_call_target="tpu_custom_call" | custom-call | tf_op jit(solution)/shard_map/pallas_call | solution.py:296
  48.8 0.7 split.12
  49.5 0.7 split.17
  50.3 0.0 copy-done.4
  50.3 0.9 convert_element_type.24
  51.3 7.1 %multiply_add_fusion = f32[48,2,128,128]{3,2,1,0:T(8,128)S(1)} fusion(f32[48,2,128,128]{3,2,1,0:T(8,128)} %param.24, f32[48,2,128]{2,1,0:T(2,128)S(1)} %mul.136, f32[48,2,128]{2,1,0:T(2,128)S(1)} %mul.134, f32[48,2,128]{2,1,0:T(2,128)S(1)} %mul.130), kind=kLoop, calls=%fused_computation | loop fusion | flops 4718592 | bytes 12730368 | tf_op jit(solution)/shard_map/add | solution.py:394
  58.5 0.0 copy-start.1
  58.5 0.0 copy-start.5
  58.5 3.0 %fusion.68 = f32[48,2,1,128]{3,2,1,0:T(1,128)S(1)} fusion(bf16[48,2,128,1]{2,3,1,0:T(2,128)(2,1)S(1)} %reshape.37, f32[48,2,128,128]{3,2,1,0:T(8,128)S(1)} %multiply_add_fusion), kind=kOutput, calls=%fused_computation.82 | convolution fusion | flops 18874368 | bytes 6365184 | tf_op jit(solution)/shard_map/bhk,bhkv->bhv/dot_general | solution.py:395
  61.4 0.0 copy-done.1
  61.4 0.1 multiply_reduce_fusion
  61.6 0.1 broadcast_multiply_fusion
  61.7 0.0 copy-done.5
  61.7 0.6 fusion.51.head
  62.4 26.5 %shard_map.231 = (f32[48,512]{1,0:T(8,128)}, bf16[384,2048]{1,0:T(8,128)(2,1)}) custom-call(bf16[48,2048]{1,0:T(8,128)(2,1)} %tokens.1, f32[1,2048]{1,0:T(1,128)} %bitcast.53, bf16[48,256]{1,0:T(8,128)(2,1)} %fusion.51.head, bf16[256,2048]{1,0:T(8,128)(2,1)} %wout.1), custom_call_target="tpu_custom_call" | custom-call | tf_op jit(solution)/shard_map/pallas_call | solution.py:296
  88.8 0.0 copy-start.3
  88.9 0.0 copy-start.2
  88.9 2.4 %fusion.16 = f32[384,256]{1,0:T(8,128)S(1)} fusion(bf16[384,2048]{1,0:T(8,128)(2,1)} %get-tuple-element.11, bf16[2,2048,256]{2,1,0:T(8,128)(2,1)} %param.36), kind=kOutput, calls=%fused_computation.21 | convolution fusion | flops 402653184 | bytes 3014656 | tf_op jit(solution)/shard_map/dot_general | solution.py:431
  91.3 0.0 copy-done.3
  91.3 0.3 dynamic-slice_reduce_fusion
  91.6 0.0 copy-done.2
  91.6 5.0 %fusion.5 = f32[384,2048]{1,0:T(8,128)} fusion(bf16[384,2048]{1,0:T(8,128)(2,1)S(1)} %copy-done.2, bf16[2,256,2048]{2,1,0:T(8,128)(2,1)} %param.38, bf16[2,2048,256]{2,1,0:T(8,128)(2,1)} %param.37, f32[384,256]{1,0:T(8,128)S(1)} %fusion.16, f32[384]{0:T(512)S(1)} %get-tuple-element.19), kind=kOutput, calls=%fused_computation.11 | convolution fusion | flops 805994496 | bytes 7210496 | tf_op jit(solution)/shard_map/dot_general | solution.py:434
  96.6 1.8 %fusion.11 = f32[384,256]{1,0:T(8,128)S(1)} fusion(bf16[384,2048]{1,0:T(8,128)(2,1)S(1)} %copy-done.2, bf16[2,2048,256]{2,1,0:T(8,128)(2,1)} %param.36), kind=kOutput, calls=%fused_computation.17 | convolution fusion | flops 402653184 | bytes 3014656 | tf_op jit(solution)/shard_map/dot_general | solution.py:431
  98.4 5.0 %fusion.6 = f32[384,2048]{1,0:T(8,128)} fusion(bf16[384,2048]{1,0:T(8,128)(2,1)S(1)} %copy-done.2, bf16[2,256,2048]{2,1,0:T(8,128)(2,1)} %param.38, bf16[2,2048,256]{2,1,0:T(8,128)(2,1)} %param.37, f32[384,256]{1,0:T(8,128)S(1)} %fusion.11, f32[384]{0:T(512)S(1)} %get-tuple-element.18), kind=kOutput, calls=%fused_computation.12 | convolution fusion | flops 805994496 | bytes 7210496 | tf_op jit(solution)/shard_map/dot_general | solution.py:434
  103.5 0.8 slice.35
  104.3 1.8 %fusion.69 = f32[384,256]{1,0:T(8,128)S(1)} fusion(bf16[384,2048]{1,0:T(8,128)(2,1)S(1)} %copy-done.2, bf16[2048,256]{1,0:T(8,128)(2,1)} %get-tuple-element.14), kind=kOutput, calls=%fused_computation.83 | convolution fusion | flops 402653184 | bytes 3014656 | tf_op jit(solution)/shard_map/dot_general | solution.py:436
  106.1 6.4 %add_convert_fusion.part = bf16[384,2048]{1,0:T(8,128)(2,1)} fusion(f32[384,2048]{1,0:T(8,128)} %fusion.5, f32[384,2048]{1,0:T(8,128)} %fusion.6, bf16[256,2048]{1,0:T(8,128)(2,1)} %get-tuple-element.16, f32[2048]{0:T(1024)S(1)} %bitcast.51, bf16[384,2048]{1,0:T(8,128)(2,1)S(1)} %copy-done.2, bf16[2048,256]{1,0:T(8,128)(2,1)} %get-tuple-element.15, ...), kind=kOutput, calls=%fused_computation.1 | convolution fusion | flops 809041920 | bytes 11935744 | tf_op jit(solution)/shard_map/dot_general | solution.py:440
  112.5 1.5 %fusion.48 = f32[48,256]{1,0:T(8,128)S(1)} fusion(bf16[2048,256]{1,0:T(8,128)(2,1)} %param.39, bf16[384,2048]{1,0:T(8,128)(2,1)S(1)} %copy-done.2, s32[]{:T(128)S(6)} %select_n.12), kind=kOutput, calls=%fused_computation.52 | convolution fusion | flops 50331648 | bytes 1294340 | tf_op jit(solution)/shard_map/dot_general | solution.py:421
  114.0 0.0 copy-done
  114.1 2.7 %convolution_convert_fusion.shared = bf16[48,2048]{1,0:T(8,128)(2,1)} fusion(bf16[256,2048]{1,0:T(8,128)(2,1)S(1)} %copy-done, bf16[2048,256]{1,0:T(8,128)(2,1)} %param.40, bf16[384,2048]{1,0:T(8,128)(2,1)S(1)} %copy-done.2, s32[]{:T(128)S(6)} %select_n.12, f32[48,256]{1,0:T(8,128)S(1)} %fusion.48), kind=kOutput, calls=%fused_computation.2 | convolution fusion | flops 100835328 | bytes 2539524 | tf_op jit(solution)/shard_map/dot_general | solution.py:424
  116.7 22.1 %shard_map.232 = bf16[48,512]{1,0:T(8,128)(2,1)} custom-call(bf16[384,2048]{1,0:T(8,128)(2,1)} %add_convert_fusion.part, bf16[48,2048]{1,0:T(8,128)(2,1)} %convolution_convert_fusion.shared, f32[48,512]{1,0:T(8,128)} %get-tuple-element.17.resid), custom_call_target="tpu_custom_call" | custom-call | tf_op jit(solution)/shard_map/pallas_call | solution.py:296
  138.8 1.4 %copy.47 = bf16[48,512]{1,0:T(8,128)(2,1)} copy(bf16[48,512]{1,0:T(8,128)(2,1)} %shard_map.232) | data formatting | bytes 98304
  (7 shorter events, 0.1 us)
Async XLA Ops:
  0.6 113.4 %copy-start = (bf16[256,2048]{1,0:T(8,128)(2,1)S(1)}, bf16[256,2048]{1,0:T(8,128)(2,1)}, u32[]{:S(2)}) copy-start(bf16[256,2048]{1,0:T(8,128)(2,1)} %param.41) | copy-start | bytes 3145732
  3.5 46.8 %copy-start.4 = (f32[256]{0:T(256)S(1)}, f32[256]{0:T(256)}, u32[]{:S(2)}) copy-start(f32[256]{0:T(256)} %param.30) | copy-start | bytes 3076
  58.5 3.0 %copy-start.1 = (f32[48,2,128,128]{3,2,1,0:T(8,128)}, f32[48,2,128,128]{3,2,1,0:T(8,128)S(1)}, u32[]{:S(2)}) copy-start(f32[48,2,128,128]{3,2,1,0:T(8,128)S(1)} %multiply_add_fusion) | copy-start | bytes 18874372
  58.5 3.3 %copy-start.5 = (f32[256]{0:T(256)S(1)}, f32[256]{0:T(256)}, u32[]{:S(2)}) copy-start(f32[256]{0:T(256)} %param.31) | copy-start | bytes 3076
  88.8 2.4 %copy-start.3 = (f32[8,48,128]{2,1,0:T(8,128)S(1)}, f32[8,48,128]{2,1,0:T(8,128)}, u32[]{:S(2)}) copy-start(f32[8,48,128]{2,1,0:T(8,128)} %get-tuple-element.12) | copy-start | bytes 589828
  88.9 2.7 %copy-start.2 = (bf16[384,2048]{1,0:T(8,128)(2,1)S(1)}, bf16[384,2048]{1,0:T(8,128)(2,1)}, u32[]{:S(2)}) copy-start(bf16[384,2048]{1,0:T(8,128)(2,1)} %get-tuple-element.11) | copy-start | bytes 4718596

commit v2 on v1

--- a/solution.py
+++ b/solution.py
@@ -54,13 +54,13 @@
     tokens, gain, route, mix, wq, wf, wi, wo = refs[:8]
     refs = refs[8:]
     if move:
-        dgate, dup, ddown = refs[:3]
-        refs = refs[3:]
+        dgate, dup = refs[:2]
+        refs = refs[2:]
     proj, route_all, mix_all = refs[:3]
     refs = refs[3:]
     if move:
-        gate_out, up_out, down_out = refs[:3]
-        refs = refs[3:]
+        gate_out, up_out = refs[:2]
+        refs = refs[2:]
     nsend, ncol, psend, precv = refs[:4]
     nsems, rsems, psems, msems = [(refs[4 + 2 * i], refs[5 + 2 * i]) for i in range(4)]
     refs = refs[12:]
@@ -87,8 +87,6 @@
         lsems = refs[2]
         rows = dgate.shape[0]
         cols = gate_out.shape[1]
-        drows = down_out.shape[0]
-        dcols = ddown.shape[1]
         locals_ = []
         for s in range(tpn):
             peer = lax.rem(tp + s, tpn)
@@ -96,7 +94,6 @@
                 (
                     (dgate.at[:, span(peer, cols)], gate_out.at[span(tp, rows), :]),
                     (dup.at[:, span(peer, cols)], up_out.at[span(tp, rows), :]),
-                    (ddown.at[span(peer, drows), :], down_out.at[:, span(tp, dcols)]),
                 )
             ):
                 if s == 0:
@@ -147,10 +144,42 @@
             copy.wait()
 
 
-def gather_kernel(
-    n, tpn, tokens, gain, head, wout, resid, moe, hsend, hrecv, sqsend, sqrecv, *sems
-):
-    hsems, qsems, esems, ysems, csems = [(sems[2 * i], sems[2 * i + 1]) for i in range(5)]
+def state_kernel(proj, bound, gain, state, new, head):
+    rows, heads, dim = state.shape[:3]
+    mixw = heads * dim
+    p = proj[...].astype(F32)
+    query, forget_pre, values, out_gate = [p[:, i * mixw : (i + 1) * mixw] for i in range(4)]
+    sig = jax.nn.sigmoid(forget_pre)
+    low = bound[...]
+    decay = low + (1.0 - low) * sig
+    keygate = (1.0 - low) * (1.0 - sig)
+    scale = gain[...] * (out_gate * jax.nn.sigmoid(out_gate))
+    for h in range(heads):
+        part = slice(h * dim, (h + 1) * dim)
+        dt, kt, qt = [jnp.transpose(a[:, part]) for a in (decay, keygate, query)]
+        reads = []
+        for b in range(rows):
+            fresh = dt[:, b : b + 1] * state[b, h] + kt[:, b : b + 1] * values[b : b + 1, part]
+            new[b, h] = fresh
+            reads.append(jnp.sum(qt[:, b : b + 1] * fresh, axis=0, keepdims=True))
+        read = jnp.concatenate(reads, axis=0)
+        read = read * lax.rsqrt(jnp.mean(read * read, axis=-1, keepdims=True) + EPS)
+        head[:, part] = (read * scale[:, part]).astype(BF16)
+
+
+def main_kernel(n, tpn, move, *refs):
+    tokens, gain, head, wout, route, mix = refs[:6]
+    hbm = refs[6:15]
+    out = refs[15]
+    moe, resid, hsend, hrecv, sqsend, sqrecv = refs[16:22]
+    held = refs[22:31]
+    part, spart, crecv, ysend, yrecv, esend, erecv = refs[31:38]
+    sems = refs[38:]
+    hsems, qsems, esems, ysems, csems, c2sems, y2sems, e2sems, wsems = [
+        (sems[2 * i], sems[2 * i + 1]) for i in range(9)
+    ]
+    lsems = sems[18]
+    egate, eup, edown, sgate, sup, sdown, dgate, dup, ddown = held
     me = lax.axis_index("ep")
     tp = lax.axis_index("tp")
     seq, width = tokens.shape
@@ -158,6 +187,7 @@
     side, core = lax.div(tp, CORES), lax.rem(tp, CORES)
     sides = tpn // CORES
     twin = side * CORES + (CORES - 1 - core)
+    exp_local = egate.shape[0]
     for t in range(tpn):
         hsend[t] = jnp.dot(
             head[...], wout[:, t * cols : (t + 1) * cols], preferred_element_type=F32
@@ -169,6 +199,15 @@
         copy = send(hsend.at[peer], hrecv.at[tp], hsems, s, {"tp": peer})
         copy.start()
         hcopies.append(copy)
+    fetches = []
+    drows = ddown.shape[0]
+    for i in range(9):
+        src, dst = hbm[i], held[i]
+        if move and i == 8:
+            src, dst = src.at[span(tp, drows), :], dst.at[:, span(tp, cols)]
+        copy = pltpu.make_async_copy(src, dst, lsems.at[i])
+        copy.start()
+        fetches.append(copy)
     total = hsend[tp].astype(F32)
     for s in range(1, tpn):
         hcopies[s - 1].wait_recv()
@@ -192,7 +231,6 @@
     def block(e, t):
         return moe.at[span(e, seq), span(t, cols)]
 
-    copies = []
     ecopies = [None]
     for s in range(1, n):
         copy = send(block(me, tp), block(me, tp), esems, s, {"ep": lax.rem(me + s, n)})
@@ -211,6 +249,15 @@
         copy = send(block(e, tp), block(e, tp), csems, s * sides, {"tp": twin})
         copy.start()
         ccopies[s, 0] = copy
+    wcopies = []
+    if move:
+        for s in range(1, tpn):
+            peer = lax.rem(tp + s, tpn)
+            copy = send(
+                hbm[8].at[span(peer, drows), :], ddown.at[:, span(tp, cols)], wsems, s, {"tp": peer}
+            )
+            copy.start()
+            wcopies.append(copy)
     for s in range(n):
         e = lax.rem(me + n - s, n)
         for q in range(1, sides):
@@ -221,69 +268,83 @@
             ccopies[s, q] = copy
     for copy in ccopies.values():
         copy.wait()
+    for copy in fetches:
+        copy.wait()
+
+    def swiglu(rows, gate, up):
+        gate_pre = jnp.dot(rows, gate, preferred_element_type=F32)
+        return gate_pre * jax.nn.sigmoid(gate_pre) * jnp.dot(rows, up, preferred_element_type=F32)
+
+    rows = moe[...]
+    lane = lax.broadcasted_iota(jnp.int32, (n * seq, route.shape[-1]), 1)
+    weights = route[...].reshape(n * seq, route.shape[-1])
+    hidden = []
+    for e in range(exp_local):
+        weight = jnp.sum(
+            jnp.where(lane == me * exp_local + e, weights, 0.0), axis=1, keepdims=True
+        )
+        hidden.append((swiglu(rows, egate[e], eup[e]) * weight).astype(BF16))
+    dense = swiglu(rows, dgate[...], dup[...]).astype(BF16)
+    shared = swiglu(moe[span(me, seq), :], sgate[...], sup[...]).astype(BF16)
+    for copy in wcopies:
+        copy.wait()
+
+    def compute(t):
+        at = span(t, cols)
+        value = mix[t, 0:1, :] * jnp.dot(dense, ddown[:, at], preferred_element_type=F32)
+        for e in range(exp_local):
+            value = value + jnp.dot(hidden[e], edown[e, :, at], preferred_element_type=F32)
+        part[t] = value.astype(BF16)
+        spart[t] = jnp.dot(shared, sdown[:, at], preferred_element_type=F32).astype(BF16)
+
+    order = list(range(1, n)) + [n, 0]
+    turns = list(range(1, sides)) + [0]
+
+    def piece(s, t):
+        if s == n:
+            return spart.at[t]
+        return part.at[t, span(lax.rem(me + s, n), seq), :]
+
+    c2, y2, e2 = {}, {}, {}
+    last = None
+    for q in turns:
+        other = lax.rem(side + q, sides) * CORES + (CORES - 1 - core)
+        compute(other)
+        for s in order:
+            i = s * sides + q
+            copy = send(piece(s, other), crecv.at[i], c2sems, i, {"tp": twin})
+            copy.start()
+            c2[s, q] = copy
+        peer = lax.rem(side + q, sides) * CORES + core
+        compute(peer)
+        for s in order:
+            i = s * sides + q
+            c2[s, q].wait_recv()
+            both = piece(s, peer)[...].astype(F32) + crecv[i].astype(F32)
+            if q:
+                ysend[i] = both.astype(BF16)
+                copy = send(ysend.at[i], yrecv.at[i], y2sems, i, {"tp": peer})
+                copy.start()
+                y2[s, q] = copy
+                continue
+            for z in turns[:-1]:
+                y2[s, z].wait_recv()
+                both = both + yrecv[i + z].astype(F32)
+            if 0 < s < n:
+                esend[s] = both.astype(BF16)
+                copy = send(esend.at[s], erecv.at[s], e2sems, s, {"ep": lax.rem(me + s, n)})
+                copy.start()
+                e2[s] = copy
+            else:
+                last = both if last is None else last + both
+    last = last + resid[...]
+    for s in range(1, n):
+        e2[s].wait_recv()
+        last = last + erecv[s].astype(F32)
+    out[...] = last.astype(BF16)
     for copy in list(ycopies.values()) + ecopies[1:] + hcopies + qcopies:
         copy.wait_send()
-
-
-def reduce_kernel(
-    n, tpn, part, shared, resid, out, crecv, ysend, yrecv, esend, erecv, *sems
-):
-    csems, ysems, esems = [(sems[2 * i], sems[2 * i + 1]) for i in range(3)]
-    me = lax.axis_index("ep")
-    tp = lax.axis_index("tp")
-    seq, cols = resid.shape
-    side, core = lax.div(tp, CORES), lax.rem(tp, CORES)
-    sides = tpn // CORES
-    twin = side * CORES + (CORES - 1 - core)
-    greet(n, tpn, me, tp)
-    order = list(range(1, n)) + [n, 0]
-
-    def block(s, t):
-        if s == n:
-            return shared.at[:, span(t, cols)]
-        return part.at[span(lax.rem(me + s, n), seq), span(t, cols)]
-
-    turns = list(range(1, sides)) + [0]
-    ccopies, ycopies, ecopies = {}, {}, {}
-    for s in order:
-        for q in turns:
-            t = lax.rem(side + q, sides) * CORES + (CORES - 1 - core)
-            i = s * sides + q
-            copy = send(block(s, t), crecv.at[i], csems, i, {"tp": twin})
-            copy.start()
-            ccopies[s, q] = copy
-    kept = {}
-    for s in order:
-        for q in turns[:-1]:
-            peer = lax.rem(side + q, sides) * CORES + core
-            i = s * sides + q
-            ccopies[s, q].wait_recv()
-            both = block(s, peer)[...].astype(F32) + crecv[i].astype(F32)
-            ysend[i] = both.astype(BF16)
-            copy = send(ysend.at[i], yrecv.at[i], ysems, i, {"tp": peer})
-            copy.start()
-            ycopies[s, q] = copy
-    last = None
-    for s in order:
-        i = s * sides
-        ccopies[s, 0].wait_recv()
-        both = block(s, tp)[...].astype(F32) + crecv[i].astype(F32)
-        for q in turns[:-1]:
-            ycopies[s, q].wait_recv()
-            both = both + yrecv[i + q].astype(F32)
-        if 0 < s < n:
-            esend[s] = both.astype(BF16)
-            copy = send(esend.at[s], erecv.at[s], esems, s, {"ep": lax.rem(me + s, n)})
-            copy.start()
-            ecopies[s] = copy
-        else:
-            last = both if last is None else last + both
-    last = last + resid[...]
-    for s in range(1, n):
-        ecopies[s].wait_recv()
-        last = last + erecv[s].astype(F32)
-    out[...] = last.astype(BF16)
-    for group in (ccopies, ycopies, ecopies):
+    for group in (c2, y2, e2):
         for copy in group.values():
             copy.wait_send()
 
@@ -368,17 +429,18 @@
     ] + pairs([n, n, n, tpn])
     spaces, out_spaces = [VM] * len(ins), [VM] * len(outs)
     if move:
-        ins += [dense_gate, dense_up, dense_down]
-        outs += [sds((width, dense_cols), BF16)] * 2 + [sds((dense_cols, width), BF16)]
-        spaces += [ANY] * 3
-        out_spaces += [ANY] * 3
-        scratch += pairs([3 * tpn]) + [pltpu.SemaphoreType.DMA((3,))]
+        ins += [dense_gate, dense_up]
+        outs += [sds((width, dense_cols), BF16)] * 2
+        spaces += [ANY] * 2
+        out_spaces += [ANY] * 2
+        scratch += pairs([2 * tpn]) + [pltpu.SemaphoreType.DMA((2,))]
     res = call(
         functools.partial(front_kernel, n, tpn, move), outs, ins, spaces, out_spaces, scratch, 0
     )
     projected, route_all, mix_all = res[:3]
     if move:
-        gate_w, up_w, down_w = res[3:]
+        gate_w, up_w = res[3:]
+        down_w = dense_down
     else:
         gate_w, up_w = [
             lax.all_to_all(w, "tp", split_axis=1, concat_axis=0, tiled=True)
@@ -386,68 +448,51 @@
         ]
         down_w = lax.all_to_all(dense_down, "tp", split_axis=0, concat_axis=1, tiled=True)
 
-    query, forget_pre, values, out_gate = jnp.split(projected.astype(F32), 4, axis=1)
-    shape = (seq, heads_local, head_dim)
-    forget_sig = jax.nn.sigmoid(forget_pre)
-    decay = (lower_bound + (1.0 - lower_bound) * forget_sig).reshape(shape)
-    keygate = ((1.0 - lower_bound) * (1.0 - forget_sig)).reshape(shape)
-    new_state = decay[..., None] * state + keygate[..., None] * values.reshape(shape)[:, :, None, :]
-    readout = jnp.einsum(
-        "bhk,bhkv->bhv", query.reshape(shape), new_state, precision=lax.Precision.HIGHEST
-    )
-    readout = readout * lax.rsqrt(jnp.mean(readout * readout, axis=-1, keepdims=True) + EPS)
-    head_out = (readout.reshape(seq, mix_local) * head_gain * jax.nn.silu(out_gate)).astype(BF16)
+    step = 8
+    new_state, head_out = pl.pallas_call(
+        state_kernel,
+        grid=(seq // step,),
+        out_shape=[sds(state.shape, F32), sds((seq, mix_local), BF16)],
+        in_specs=[
+            pl.BlockSpec((step, 4 * mix_local), lambda i: (i, 0)),
+            pl.BlockSpec((1, mix_local), lambda i: (0, 0)),
+            pl.BlockSpec((1, mix_local), lambda i: (0, 0)),
+            pl.BlockSpec((step,) + state.shape[1:], lambda i: (i, 0, 0, 0)),
+        ],
+        out_specs=[
+            pl.BlockSpec((step,) + state.shape[1:], lambda i: (i, 0, 0, 0)),
+            pl.BlockSpec((step, mix_local), lambda i: (i, 0)),
+        ],
+    )(projected, lower_bound[None, :], head_gain[None, :], state)
 
     sides = tpn // CORES
-    resid, moe_in = call(
-        functools.partial(gather_kernel, n, tpn),
-        [sds((seq, cols), F32), sds((n * seq, width), BF16)],
-        [tokens, ffn_gain[None, :], head_out, w_output],
-        [VM] * 4,
-        [VM] * 2,
+    blocks = (n + 1) * sides
+    big = [expert_gate, expert_up, expert_down, shared_gate, shared_up, shared_down]
+    big += [gate_w, up_w, down_w]
+    held = [VM(w.shape, BF16) for w in big]
+    if move:
+        held[8] = VM((dense_cols, width), BF16)
+    (mixed,) = call(
+        functools.partial(main_kernel, n, tpn, move),
+        [sds((seq, cols), BF16)],
+        [tokens, ffn_gain[None, :], head_out, w_output, route_all, mix_all] + big,
+        [VM] * 6 + [ANY] * 9,
+        [VM],
         [
+            VM((n * seq, width), BF16),
+            VM((seq, cols), F32),
             VM((tpn, seq, cols), BF16),
             VM((tpn, seq, cols), BF16),
             VM((seq, LANES), F32),
             VM((tpn, seq, LANES), F32),
         ]
-        + pairs([tpn, tpn, n, n * sides, n * sides]),
+        + held
+        + [VM((tpn, n * seq, cols), BF16), VM((tpn, seq, cols), BF16)]
+        + [VM((blocks, seq, cols), BF16)] * 3
+        + [VM((n, seq, cols), BF16)] * 2
+        + pairs([tpn, tpn, n, n * sides, n * sides, blocks, blocks, n, tpn])
+        + [pltpu.SemaphoreType.DMA((9,))],
         1,
-    )
-
-    ep_index = lax.axis_index("ep")
-    own = lax.dynamic_slice_in_dim(moe_in, ep_index * seq, seq, 0)
-    shared_hidden = (
-        jax.nn.silu(jnp.dot(own, shared_gate, preferred_element_type=F32))
-        * jnp.dot(own, shared_up, preferred_element_type=F32)
-    ).astype(BF16)
-    shared_part = jnp.dot(shared_hidden, shared_down, preferred_element_type=F32).astype(BF16)
-
-    route_rows = lax.dynamic_slice_in_dim(
-        route_all.reshape(n * seq, slots), ep_index * exp_local, exp_local, 1
-    )
-    part = jnp.zeros((n * seq, width), F32)
-    for e in range(exp_local):
-        gate_pre = jnp.dot(moe_in, expert_gate[e], preferred_element_type=F32)
-        up_pre = jnp.dot(moe_in, expert_up[e], preferred_element_type=F32)
-        hidden = (jax.nn.silu(gate_pre) * up_pre * route_rows[:, e : e + 1]).astype(BF16)
-        part = part + jnp.dot(hidden, expert_down[e], preferred_element_type=F32)
-    dense_hidden = (
-        jax.nn.silu(jnp.dot(moe_in, gate_w, preferred_element_type=F32))
-        * jnp.dot(moe_in, up_w, preferred_element_type=F32)
-    ).astype(BF16)
-    mix_row = mix_all[:, 0, :].reshape(1, width)
-    part = part + mix_row * jnp.dot(dense_hidden, down_w, preferred_element_type=F32)
-    blocks = (n + 1) * sides
-    (mixed,) = call(
-        functools.partial(reduce_kernel, n, tpn),
-        [sds((seq, cols), BF16)],
-        [part.astype(BF16), shared_part, resid],
-        [VM] * 3,
-        [VM],
-        [VM((blocks, seq, cols), BF16)] * 3 + [VM((n, seq, cols), BF16)] * 2
-        + pairs([blocks, blocks, n]),
-        2,
     )
     return (mixed, new_state)
 

time: 141 us -> 103 us (0.73)
  matrix products: 29.6 us -> 0 us
  other arithmetic: 11.1 us -> 2.11 us
  Pallas kernels: 93.9 us -> 97.9 us
  local copies, waits for them, and re-layouts: 4.81 us -> 2.04 us
    dot_general x9 -> x0, matrix products: 29.6 us -> none  [the longest x2 10 us: local(): part = part + jnp.dot(hidden, expert_down[e], preferred_element_type=F32)]
    pallas_call x0 -> x1, Pallas kernels: none -> 10.1 us  [local(): pl.pallas_call(state_kernel, grid=(seq // step,), out_shape=[sds(state.sh...]
    add x2 -> x0, other arithmetic: 7.14 us -> none  [the longest x1 7.12 us: local(): decay[..., None] * state]
    pallas_call x3 -> x2, Pallas kernels: 93.9 us -> 87.7 us  [call(): pl.pallas_call(kernel, out_shape=outs, in_specs=[pl.BlockSpec(memory_spac...]
    convert_element_type x2 -> x0, other arithmetic: 1.54 us -> none  [the longest x1 0.91 us: local(): projected.astype(F32)]
    split x2 -> x0, local copies, waits for them, and re-layouts: 1.48 us -> none  [local(): jnp.split(projected.astype(F32), 4, axis=1)]
where the time goes in v2:
time: 103 us
  Pallas kernels  97.9 us (95%)
  other arithmetic  2.11 us (2%)
  local copies, waits for them, and re-layouts  2.04 us (2%)
    pallas_call x2, Pallas kernels, call(): pl.pallas_call(kernel, out_shape=outs, in_specs=[pl.BlockSpec(memory_spac...  87.7 us
    pallas_call x1, Pallas kernels, local(): pl.pallas_call(state_kernel, grid=(seq // step,), out_shape=[sds(state.sh...  10.1 us

profile of v2, /device:TPU:0, one launch (start us, length us, event | category | flops | bytes accessed | tf_op | source)
XLA Modules:
  0.0 102.7 jit_solution(1547998428092244278)
XLA Ops:
  0.6 0.7 add_divide_fusion
  1.3 0.6 broadcast_in_dim.37.refs_3_
  1.9 1.4 %select_reduce_fusion.refs_2_ = f32[48,128]{1,0:T(8,128)} fusion(f32[48,4]{0,1:T(4,128)} %param.35, s32[48,4]{0,1:T(4,128)} %param.34), kind=kLoop, calls=%fused_computation | loop fusion | flops 67584 | bytes 26112 | tf_op jit(solution)/shard_map/reduce_sum | solution.py:407
  3.4 35.8 %shard_map.230 = (bf16[48,1024]{1,0:T(8,128)(2,1)}, f32[8,48,128]{2,1,0:T(8,128)}, f32[4,8,512]{2,1,0:T(8,128)}, bf16[2048,256]{1,0:T(8,128)(2,1)}, bf16[2048,256]{1,0:T(8,128)(2,1)}) custom-call(bf16[48,2048]{1,0:T(8,128)(2,1)} %refs_0_.3, f32[1,2048]{1,0:T(1,128)} %bitcast.4, f32[48,128]{1,0:T(8,128)} %select_reduce_fusion.refs_2_, ...), custom_call_target="tpu_custom_call" | custom-call | tf_op jit(solution)/shard_map/pallas_call | solution.py:357
  39.2 10.1 %shard_map.231 = (f32[48,2,128,128]{3,2,1,0:T(8,128)}, bf16[48,256]{1,0:T(8,128)(2,1)}) custom-call(bf16[48,1024]{1,0:T(8,128)(2,1)} %get-tuple-element.9.proj, f32[1,256]{1,0:T(1,128)} %bitcast.6, f32[1,256]{1,0:T(1,128)} %bitcast.7, f32[48,2,128,128]{3,2,1,0:T(8,128)} %state.1), custom_call_target="tpu_custom_call" | custom-call | tf_op jit(solution)/shard_map/pallas_call | solution.py:452
  49.3 52.0 %shard_map.232 = bf16[48,512]{1,0:T(8,128)(2,1)} custom-call(bf16[48,2048]{1,0:T(8,128)(2,1)} %refs_0_.3, f32[1,2048]{1,0:T(1,128)} %bitcast.5, bf16[48,256]{1,0:T(8,128)(2,1)} %get-tuple-element.10.refs_2_, bf16[256,2048]{1,0:T(8,128)(2,1)} %refs_3_.1, f32[8,48,128]{2,1,0:T(8,128)} %get-tuple-element.11.refs_4_, f32[4,8,512]{2,1,0:T(8,128)} %get-tuple-element.12.refs_5_, ...), custom_call_target="tpu_custom_call" | custom-call | tf_op jit(solution)/shard_map/pallas_call | solution.py:357
  101.2 1.4 %copy.28 = bf16[48,512]{1,0:T(8,128)(2,1)} copy(bf16[48,512]{1,0:T(8,128)(2,1)} %shard_map.232) | data formatting | bytes 98304

commit v3 on v2

--- a/solution.py
+++ b/solution.py
@@ -29,6 +29,19 @@
 
 def span(index, size):
     return pl.ds(pl.multiple_of(index * size, size), size)
+
+
+def ring(n, me):
+    half = n // 2
+    z, x = lax.div(me, 2), lax.rem(me, 2)
+
+    def peer(s, f):
+        return lax.rem(z + s, half) * 2 + lax.rem(x + f, 2)
+
+    def source(s, f):
+        return lax.rem(z + half - s, half) * 2 + lax.rem(x + f, 2)
+
+    return half, peer, source, source(0, 1)
 
 
 def greet(n, tpn, me, tp):
@@ -51,8 +64,8 @@
 
 
 def front_kernel(n, tpn, move, *refs):
-    tokens, gain, route, mix, wq, wf, wi, wo = refs[:8]
-    refs = refs[8:]
+    tokens, gain, ids, weight, premix, wq, wf, wi, wo = refs[:9]
+    refs = refs[9:]
     if move:
         dgate, dup = refs[:2]
         refs = refs[2:]
@@ -61,9 +74,9 @@
     if move:
         gate_out, up_out = refs[:2]
         refs = refs[2:]
-    nsend, ncol, psend, precv = refs[:4]
-    nsems, rsems, psems, msems = [(refs[4 + 2 * i], refs[5 + 2 * i]) for i in range(4)]
-    refs = refs[12:]
+    route, mix, nsend, ncol, psend, precv, xrecv = refs[:7]
+    nsems, rsems, psems, msems, xsems = [(refs[7 + 2 * i], refs[8 + 2 * i]) for i in range(5)]
+    refs = refs[17:]
     me = lax.axis_index("ep")
     tp = lax.axis_index("tp")
     seq = tokens.shape[0]
@@ -75,13 +88,22 @@
     ).astype(BF16)
     for d in range(n):
         nsend[d] = normed[:, d * depth : (d + 1) * depth]
+    lane = lax.broadcasted_iota(jnp.int32, route.shape, 1)
+    table = jnp.zeros(route.shape, F32)
+    for k in range(ids.shape[1]):
+        table = table + jnp.where(lane == ids[:, k : k + 1], weight[:, k : k + 1], 0.0)
+    route[...] = table
+    mix[...] = jnp.broadcast_to(jax.nn.sigmoid(premix[...]), mix.shape)
+    half, to, source, mate = ring(n, me)
     greet(n, tpn, me, tp)
-    ncopies, others = [None], []
-    for s in range(1, n):
-        peer = lax.rem(me + s, n)
-        copy = send(nsend.at[peer], ncol.at[me], nsems, s, {"ep": peer})
-        copy.start()
-        ncopies.append(copy)
+    ncopies, others = {}, []
+    for f in (1, 0):
+        for s in list(range(1, half)) + [0]:
+            if s or f:
+                peer = to(s, f)
+                copy = send(nsend.at[peer], ncol.at[me], nsems, 2 * s + f, {"ep": peer})
+                copy.start()
+                ncopies[s, f] = copy
     if move:
         wsems = (refs[0], refs[1])
         lsems = refs[2]
@@ -120,23 +142,35 @@
             for w in (wq, wf, wi, wo)
         ]
 
-    pcopies = [None]
-    for s in range(1, n):
-        source = lax.rem(me + n - s, n)
-        ncopies[s].wait_recv()
-        for i, part in enumerate(project(ncol[source])):
-            psend[source, :, i * mixw : (i + 1) * mixw] = part
-        copy = send(psend.at[source], precv.at[me], psems, s, {"ep": source})
-        copy.start()
-        pcopies.append(copy)
-    own = jnp.concatenate(project(nsend[me]), axis=1).astype(F32)
-    for s in range(1, n):
+    pcopies, xcopies = {}, {}
+    turns = list(range(1, half)) + [0]
+    for s in turns:
+        d = source(s, 1)
+        ncopies[s, 1].wait_recv()
+        for i, part in enumerate(project(ncol[d])):
+            psend[d, :, i * mixw : (i + 1) * mixw] = part
+        copy = send(psend.at[d], xrecv.at[s], xsems, s, {"ep": mate})
+        copy.start()
+        xcopies[s] = copy
+    for s in turns:
+        d = source(s, 0)
+        if s:
+            ncopies[s, 0].wait_recv()
+        own = jnp.concatenate(project(ncol[d] if s else nsend[me]), axis=1).astype(F32)
+        xcopies[s].wait_recv()
+        own = own + xrecv[s].astype(F32)
+        if s:
+            psend[d] = own.astype(BF16)
+            copy = send(psend.at[d], precv.at[s], psems, s, {"ep": d})
+            copy.start()
+            pcopies[s] = copy
+    for s in range(1, half):
         pcopies[s].wait_recv()
-        own = own + precv[lax.rem(me + s, n)].astype(F32)
+        own = own + precv[s].astype(F32)
     proj[...] = own.astype(BF16)
-    for s in range(1, n):
-        ncopies[s].wait_send()
-        pcopies[s].wait_send()
+    for group in (ncopies, xcopies, pcopies):
+        for copy in group.values():
+            copy.wait_send()
     for copy in others:
         copy.wait()
     if move:
@@ -173,12 +207,12 @@
     out = refs[15]
     moe, resid, hsend, hrecv, sqsend, sqrecv = refs[16:22]
     held = refs[22:31]
-    part, spart, crecv, ysend, yrecv, esend, erecv = refs[31:38]
-    sems = refs[38:]
-    hsems, qsems, esems, ysems, csems, c2sems, y2sems, e2sems, wsems = [
-        (sems[2 * i], sems[2 * i + 1]) for i in range(9)
+    part, spart, crecv, ysend, yrecv, esend, erecv, xrecv = refs[31:39]
+    sems = refs[39:]
+    hsems, qsems, esems, ysems, csems, c2sems, y2sems, e2sems, wsems, xsems, x2sems = [
+        (sems[2 * i], sems[2 * i + 1]) for i in range(11)
     ]
-    lsems = sems[18]
+    lsems = sems[22]
     egate, eup, edown, sgate, sup, sdown, dgate, dup, ddown = held
     me = lax.axis_index("ep")
     tp = lax.axis_index("tp")
@@ -231,24 +265,35 @@
     def block(e, t):
         return moe.at[span(e, seq), span(t, cols)]
 
-    ecopies = [None]
-    for s in range(1, n):
-        copy = send(block(me, tp), block(me, tp), esems, s, {"ep": lax.rem(me + s, n)})
-        copy.start()
-        ecopies.append(copy)
-    ycopies, ccopies = {}, {}
-    for s in range(n):
-        e = lax.rem(me + n - s, n)
+    half, to, source, mate = ring(n, me)
+    ecopies, xcopies, ycopies, ccopies = {}, {}, {}, {}
+    for s in range(1, half):
+        copy = send(block(me, tp), block(me, tp), esems, s, {"ep": to(s, 0)})
+        copy.start()
+        ecopies[s] = copy
+
+    def spread(s, f):
+        e, u = source(s, f), 2 * s + f
+        for q in range(1, sides):
+            peer = lax.rem(side + q, sides) * CORES + core
+            copy = send(block(e, tp), block(e, tp), ysems, u * sides + q, {"tp": peer})
+            copy.start()
+            ycopies[u, q] = copy
+        copy = send(block(e, tp), block(e, tp), csems, u * sides, {"tp": twin})
+        copy.start()
+        ccopies[u, 0] = copy
+
+    for s in range(half):
+        e = source(s, 0)
         if s:
             ecopies[s].wait_recv()
-        for q in range(1, sides):
-            peer = lax.rem(side + q, sides) * CORES + core
-            copy = send(block(e, tp), block(e, tp), ysems, s * sides + q, {"tp": peer})
-            copy.start()
-            ycopies[s, q] = copy
-        copy = send(block(e, tp), block(e, tp), csems, s * sides, {"tp": twin})
-        copy.start()
-        ccopies[s, 0] = copy
+        copy = send(block(e, tp), block(e, tp), xsems, s, {"ep": mate})
+        copy.start()
+        xcopies[s] = copy
+        spread(s, 0)
+    for s in range(half):
+        xcopies[s].wait_recv()
+        spread(s, 1)
     wcopies = []
     if move:
         for s in range(1, tpn):
@@ -258,14 +303,14 @@
             )
             copy.start()
             wcopies.append(copy)
-    for s in range(n):
-        e = lax.rem(me + n - s, n)
+    for u in [2 * s for s in range(half)] + [2 * s + 1 for s in range(half)]:
+        e = source(u // 2, u % 2)
         for q in range(1, sides):
-            ycopies[s, q].wait_recv()
+            ycopies[u, q].wait_recv()
             t = lax.rem(side + sides - q, sides) * CORES + core
-            copy = send(block(e, t), block(e, t), csems, s * sides + q, {"tp": twin})
+            copy = send(block(e, t), block(e, t), csems, u * sides + q, {"tp": twin})
             copy.start()
-            ccopies[s, q] = copy
+            ccopies[u, q] = copy
     for copy in ccopies.values():
         copy.wait()
     for copy in fetches:
@@ -297,15 +342,16 @@
         part[t] = value.astype(BF16)
         spart[t] = jnp.dot(shared, sdown[:, at], preferred_element_type=F32).astype(BF16)
 
-    order = list(range(1, n)) + [n, 0]
+    order = [2 * s + 1 for s in list(range(1, half)) + [0]]
+    order += [2 * s for s in range(1, half)] + [n, 0]
     turns = list(range(1, sides)) + [0]
 
     def piece(s, t):
         if s == n:
             return spart.at[t]
-        return part.at[t, span(lax.rem(me + s, n), seq), :]
-
-    c2, y2, e2 = {}, {}, {}
+        return part.at[t, span(to(s // 2, s % 2), seq), :]
+
+    c2, y2, e2, x2 = {}, {}, {}, {}
     last = None
     for q in turns:
         other = lax.rem(side + q, sides) * CORES + (CORES - 1 - core)
@@ -330,21 +376,30 @@
             for z in turns[:-1]:
                 y2[s, z].wait_recv()
                 both = both + yrecv[i + z].astype(F32)
-            if 0 < s < n:
+            far = s // 2
+            if s < n and s % 2 == 0:
+                x2[far].wait_recv()
+                both = both + xrecv[far].astype(F32)
+            if s < n and s % 2:
                 esend[s] = both.astype(BF16)
-                copy = send(esend.at[s], erecv.at[s], e2sems, s, {"ep": lax.rem(me + s, n)})
+                copy = send(esend.at[s], xrecv.at[far], x2sems, far, {"ep": mate})
                 copy.start()
-                e2[s] = copy
+                x2[far] = copy
+            elif 0 < s < n:
+                esend[s] = both.astype(BF16)
+                copy = send(esend.at[s], erecv.at[far], e2sems, far, {"ep": to(far, 0)})
+                copy.start()
+                e2[far] = copy
             else:
                 last = both if last is None else last + both
     last = last + resid[...]
-    for s in range(1, n):
+    for s in range(1, half):
         e2[s].wait_recv()
         last = last + erecv[s].astype(F32)
     out[...] = last.astype(BF16)
-    for copy in list(ycopies.values()) + ecopies[1:] + hcopies + qcopies:
+    for copy in hcopies + qcopies:
         copy.wait_send()
-    for group in (c2, y2, e2):
+    for group in (ycopies, ecopies, xcopies, c2, y2, e2, x2):
         for copy in group.values():
             copy.wait_send()
 
@@ -404,29 +459,25 @@
     sds = jax.ShapeDtypeStruct
     VM, ANY = pltpu.VMEM, pl.ANY
 
-    route = jnp.sum(
-        jnp.where(
-            route_ids[:, :, None] == jnp.arange(slots, dtype=jnp.int32)[None, None, :],
-            route_weight[:, :, None],
-            jnp.float32(0.0),
-        ),
-        axis=1,
-    )
-    mix = jnp.broadcast_to(jax.nn.sigmoid(dense_mix)[None, :], (8, cols))
     dense_cols = dense_gate.shape[1] // tpn
     move = dense_cols % LANES == 0
-    ins = [tokens, norm_gain[None, :], route, mix, w_query, w_forget, w_input, w_outgate]
+    ins = [tokens, norm_gain[None, :], route_ids, route_weight, dense_mix[None, :]]
+    ins += [w_query, w_forget, w_input, w_outgate]
     outs = [
         sds((seq, 4 * mix_local), BF16),
         sds((n, seq, slots), F32),
         sds((tpn, 8, cols), F32),
     ]
+    half = n // 2
     scratch = [
+        VM((seq, slots), F32),
+        VM((8, cols), F32),
         VM((n, seq, depth), BF16),
         VM((n, seq, depth), BF16),
         VM((n, seq, 4 * mix_local), BF16),
-        VM((n, seq, 4 * mix_local), BF16),
-    ] + pairs([n, n, n, tpn])
+        VM((half, seq, 4 * mix_local), BF16),
+        VM((half, seq, 4 * mix_local), BF16),
+    ] + pairs([n, n, half, tpn, half])
     spaces, out_spaces = [VM] * len(ins), [VM] * len(outs)
     if move:
         ins += [dense_gate, dense_up]
@@ -489,8 +540,9 @@
         + held
         + [VM((tpn, n * seq, cols), BF16), VM((tpn, seq, cols), BF16)]
         + [VM((blocks, seq, cols), BF16)] * 3
-        + [VM((n, seq, cols), BF16)] * 2
-        + pairs([tpn, tpn, n, n * sides, n * sides, blocks, blocks, n, tpn])
+        + [VM((n, seq, cols), BF16)]
+        + [VM((half, seq, cols), BF16)] * 2
+        + pairs([tpn, tpn, half, n * sides, n * sides, blocks, blocks, half, tpn, half, half])
         + [pltpu.SemaphoreType.DMA((9,))],
         1,
     )

time: 103 us -> 100 us (0.971)
  Pallas kernels: 97.9 us -> 94.9 us
  local copies, waits for them, and re-layouts: 2.04 us -> 4.17 us
  other arithmetic: 2.11 us -> 0 us
    pallas_call x2, Pallas kernels: 87.7 us -> 84.7 us  [call(): pl.pallas_call(kernel, out_shape=outs, in_specs=[pl.BlockSpec(memory_spac...]
    unnamed x1 -> x3, local copies, waits for them, and re-layouts: 1.42 us -> 4.17 us
    reduce_sum x1 -> x0, other arithmetic: 1.43 us -> none  [local(): jnp.sum(jnp.where(route_ids[:, :, None] == jnp.arange(slots, dtype=jnp.in...]
where the time goes in v3:
time: 100 us; the launch traced here: 99.7 us
  Pallas kernels  94.9 us (95%)
  local copies, waits for them, and re-layouts  4.17 us (4%)
    pallas_call x2, Pallas kernels, call(): pl.pallas_call(kernel, out_shape=outs, in_specs=[pl.BlockSpec(memory_spac...  84.7 us
    pallas_call x1, Pallas kernels, local(): pl.pallas_call(state_kernel, grid=(seq // step,), out_shape=[sds(state.sh...  10.1 us
    unnamed x3, local copies, waits for them, and re-layouts  4.17 us

profile of v3, /device:TPU:0, one launch (start us, length us, event | category | flops | bytes accessed | tf_op | source)
XLA Modules:
  0.0 99.7 jit_solution(1849453050893048462)
XLA Ops:
  0.6 1.4 %copy.25.refs_2_ = s32[48,4]{1,0:T(8,128)} copy(s32[48,4]{0,1:T(4,128)} %param.34) | data formatting | bytes 1536 | tf_op args[11]
  2.0 1.4 %copy.26.refs_3_ = f32[48,4]{1,0:T(8,128)} copy(f32[48,4]{0,1:T(4,128)} %param.35) | data formatting | bytes 1536 | tf_op args[12]
  3.4 34.0 %shard_map.230 = (bf16[48,1024]{1,0:T(8,128)(2,1)}, f32[8,48,128]{2,1,0:T(8,128)}, f32[4,8,512]{2,1,0:T(8,128)}, bf16[2048,256]{1,0:T(8,128)(2,1)}, bf16[2048,256]{1,0:T(8,128)(2,1)}) custom-call(bf16[48,2048]{1,0:T(8,128)(2,1)} %refs_0_.3, f32[1,2048]{1,0:T(1,128)} %bitcast.5, s32[48,4]{1,0:T(8,128)} %copy.25.refs_2_, f32[48,4]{1,0:T(8,128)} %copy.26.refs_3_, ...), custom_call_target="tpu_custom_call" | custom-call | tf_op jit(solution)/shard_map/pallas_call | solution.py:412
  37.4 10.1 %shard_map.231 = (f32[48,2,128,128]{3,2,1,0:T(8,128)}, bf16[48,256]{1,0:T(8,128)(2,1)}) custom-call(bf16[48,1024]{1,0:T(8,128)(2,1)} %get-tuple-element.9.proj, f32[1,256]{1,0:T(1,128)} %bitcast.8, f32[1,256]{1,0:T(1,128)} %bitcast.9, f32[48,2,128,128]{3,2,1,0:T(8,128)} %state.1), custom_call_target="tpu_custom_call" | custom-call | tf_op jit(solution)/shard_map/pallas_call | solution.py:503
  47.5 50.7 %shard_map.232 = bf16[48,512]{1,0:T(8,128)(2,1)} custom-call(bf16[48,2048]{1,0:T(8,128)(2,1)} %refs_0_.3, f32[1,2048]{1,0:T(1,128)} %bitcast.6, bf16[48,256]{1,0:T(8,128)(2,1)} %get-tuple-element.10.refs_2_, bf16[256,2048]{1,0:T(8,128)(2,1)} %refs_3_.2, f32[8,48,128]{2,1,0:T(8,128)} %get-tuple-element.11.refs_4_, f32[4,8,512]{2,1,0:T(8,128)} %get-tuple-element.12.refs_5_, ...), custom_call_target="tpu_custom_call" | custom-call | tf_op jit(solution)/shard_map/pallas_call | solution.py:412
  98.3 1.4 %copy.28 = bf16[48,512]{1,0:T(8,128)(2,1)} copy(bf16[48,512]{1,0:T(8,128)(2,1)} %shard_map.232) | data formatting | bytes 98304
